TPU v7x, 256 devices: a whole 4x4x8 slice. The times are simulated.
256 devices in a mesh: sp: 64 (over z, y, core), tp: 4 (over x).
Axes of the slice: x: 4, y: 4, z: 8, core: 2. Of those that a mesh axis runs over, the one named last changes fastest.
Arguments:
- tokens: bfloat16 [10240, 2048], P('sp'), may hold values from -6 to 6
- input_gain: float32 [2048], replicated, may hold values from 0.1 to 1.9
- chain_query: bfloat16 [2048, 1024], P('sp', 'tp'), may hold values from -0.125 to 0.125
- forward_gate: bfloat16 [2048, 1024], P('sp', 'tp'), may hold values from -0.125 to 0.125
- backward_gate: bfloat16 [2048, 1024], P('sp', 'tp'), may hold values from -0.125 to 0.125
- chain_value: bfloat16 [2048, 1024], P('sp', 'tp'), may hold values from -0.125 to 0.125
- output_gate: bfloat16 [2048, 1024], P('sp', 'tp'), may hold values from -0.125 to 0.125
- forget_rate: float32 [2, 1024], P(None, 'tp'), may hold values from 0.2 to 6
- chain_gain: float32 [1024], P('tp'), may hold values from 0.1 to 1.9
- query_down: bfloat16 [2048, 768], P('sp'), may hold values from -0.125 to 0.125
- latent_down: bfloat16 [2048, 512], P('sp'), may hold values from -0.125 to 0.125
- rotary_down: bfloat16 [2048, 64], replicated, may hold values from -0.125 to 0.125
- query_latent_gain: float32 [768], replicated, may hold values from 0.1 to 1.9
- latent_gain: float32 [512], replicated, may hold values from 0.1 to 1.9
- query_up: bfloat16 [768, 1536], P(None, 'tp'), may hold values from -0.21875 to 0.21875
- latent_up: bfloat16 [512, 2048], P(None, 'tp'), may hold values from -0.25 to 0.25
- query_head_gain: float32 [192], replicated, may hold values from 0.1 to 1.9
- key_head_gain: float32 [192], replicated, may hold values from 0.1 to 1.9
- mixer_gain: float32 [1024], P('tp'), may hold values from 0.1 to 1.9
- chain_out: bfloat16 [1024, 2048], P('tp', 'sp'), may hold values from -0.125 to 0.125
- attend_out: bfloat16 [1024, 2048], P('tp', 'sp'), may hold values from -0.125 to 0.125
Outputs:
- mixed: float32 [10240, 2048], P(('sp', 'tp'))
All inputs are finite; a program needn't handle non-finite values.
Results may differ from a plain program's by a relative error of at most 0.017.
Values may be sent and summed in bfloat16 or wider, within the bound.
No kernel may reach another device: no remote copies, remote signals or barrier semaphores. Data moves between devices by JAX's collectives and lax.ppermute only.
A program may use at most 128 MiB of HBM per device.

v0:
```python
import jax
import jax.numpy as jnp
from jax import lax
from jax.sharding import Mesh
from jax.sharding import PartitionSpec as P

KEY_DIM = 128
VAL_DIM = 128
NOPE_DIM = 128
ROPE_DIM = 64
VHEAD_DIM = 128
ATT_QK = 192
SP = ("sp_0", "sp_1", "sp_2")
SP_TP = ("sp_0", "sp_1", "sp_2", "tp")
norm_eps = 1e-06
rope_theta = 10000.0
finest_arithmetic_mode = lax.Precision.HIGHEST


def turned_gather(arrays, axis, dims):
    turned = [jnp.moveaxis(a, dim, 0) for a, dim in zip(arrays, dims)]
    both = jnp.concatenate([t.reshape(len(t), -1) for t in turned], axis=1)
    filled, at, done = (lax.all_gather(both, axis, axis=0, tiled=True), 0, [])
    for t, dim in zip(turned, dims):
        share = filled[:, at : at + t[0].size].reshape(-1, *t.shape[1:])
        done.append(jnp.moveaxis(share, 0, dim))
        at += t[0].size
    return tuple(done)


def filled_with(value, identity):
    return jax.tree.map(
        lambda part, zero: jnp.zeros_like(part) + jnp.asarray(zero, part.dtype), value, identity
    )


def carried_in(value, axes, combine, identity, reverse):
    before = start = filled_with(value, identity)
    total = value
    for axis in reversed(axes):
        count, position = (lax.axis_size(axis), lax.axis_index(axis))
        pieces = jax.tree.map(lambda part: lax.all_gather(part, axis), total)
        inside, total = (start, start)
        for k in reversed(range(count)) if reverse else range(count):
            passed = k > position if reverse else k < position
            total = combine(total, jax.tree.map(lambda part: part[k], pieces))
            inside = jax.tree.map(lambda new, old: jnp.where(passed, new, old), total, inside)
        before = combine(inside, before)
    return before


def side_by_side(arrays, axis, dim, along):
    ends, at = ([], 0)
    for a in arrays[:-1]:
        at += a.shape[along]
        ends.append(at)
    both = jnp.concatenate(arrays, axis=along)
    return tuple(jnp.split(lax.all_gather(both, axis, axis=dim, tiled=True), ends, axis=along))


def in_blocks(value, dim, count):
    before, after = (value.shape[:dim], value.shape[dim + 1 :])
    return jnp.moveaxis(value.reshape(*before, count, -1, *after), dim, 0)


def sent_and_summed(value, axis, dim):
    count = lax.axis_size(axis)
    pieces = lax.all_to_all(in_blocks(value, dim, count), axis, 0, 0, tiled=True)
    return jnp.sum(pieces, axis=0)


def rms_scale(values, gain_vec):
    mean_square = jnp.mean(values * values, axis=-1, keepdims=True)
    return values * lax.rsqrt(mean_square + norm_eps) * gain_vec


def rotate_tail(values, positions):
    half_dim = ROPE_DIM // 2
    inverse = rope_theta ** (-jnp.arange(0, ROPE_DIM, 2).astype(jnp.float32) / ROPE_DIM)
    angles = positions.astype(jnp.float32)[:, None] * inverse
    cosine = jnp.cos(angles)[:, None, :]
    sine_table = jnp.sin(angles)[:, None, :]
    unrotated = values[..., :NOPE_DIM]
    first_half = values[..., NOPE_DIM : NOPE_DIM + half_dim]
    latter_element = values[..., NOPE_DIM + half_dim :]
    return jnp.concatenate(
        [
            unrotated,
            first_half * cosine - latter_element * sine_table,
            latter_element * cosine + first_half * sine_table,
        ],
        axis=-1,
    )


def gate_parts(pre_gate, rate_row, seq_len):
    opening = rate_row / seq_len * jax.nn.sigmoid(-pre_gate.astype(jnp.float32))
    return (jnp.log1p(-opening), opening)


def summarize(query_rows, key_rows, payload_array_lines, log_decay):
    cumulative = jnp.cumsum(log_decay, axis=0)
    weighted_probe_vectors = query_rows * jnp.exp(cumulative)
    weighted_lookup_vectors = key_rows * jnp.exp(-cumulative)
    overall_shrink_multiplier = jnp.exp(cumulative[-1])
    recurrent_memory_digest = overall_shrink_multiplier[:, :, None] * jnp.einsum(
        "jre,jrw->rew",
        weighted_lookup_vectors,
        payload_array_lines,
        precision=finest_arithmetic_mode,
    )
    return (
        weighted_probe_vectors,
        weighted_lookup_vectors,
        overall_shrink_multiplier,
        recurrent_memory_digest,
    )


def emit(weighted_probe_vectors, weighted_lookup_vectors, payload_array_lines, incoming_update):
    length = weighted_probe_vectors.shape[0]
    lower_mask = jnp.tril(jnp.ones((length, length), jnp.float32))
    scores = (
        jnp.einsum(
            "thk,shk->hts",
            weighted_probe_vectors,
            weighted_lookup_vectors,
            precision=finest_arithmetic_mode,
        )
        * lower_mask
    )
    within = jnp.einsum(
        "hts,shv->thv", scores, payload_array_lines, precision=finest_arithmetic_mode
    )
    prior_state = jnp.einsum(
        "mjf,jfi->mji", weighted_probe_vectors, incoming_update, precision=finest_arithmetic_mode
    )
    return within + prior_state


def chain_combine(earlier, following):
    return (earlier[0] * following[0], following[0][:, :, None] * earlier[1] + following[1])


def add_scores(running, query_final, key_piece, value_piece):
    score_scale = query_final.shape[-1] ** (-0.5)
    scores = (
        jnp.einsum("qhd,khd->hqk", query_final, key_piece, preferred_element_type=jnp.float32)
        * score_scale
    )
    weights = jnp.exp(scores)
    numerator = running[0] + jnp.einsum(
        "hqk,khv->qhv",
        weights.astype(jnp.bfloat16),
        value_piece,
        preferred_element_type=jnp.float32,
    )
    return (numerator, running[1] + jnp.sum(weights, axis=-1))


def on_device(
    tokens,
    input_gain,
    chain_query,
    forward_gate,
    backward_gate,
    chain_value,
    output_gate,
    forget_rate,
    chain_gain,
    query_down,
    latent_down,
    rotary_down,
    query_latent_gain,
    latent_gain,
    query_up,
    latent_up,
    query_head_gain,
    key_head_gain,
    mixer_gain,
    chain_out,
    attend_out,
):
    gathered = turned_gather(
        (
            chain_query,
            forward_gate,
            backward_gate,
            chain_value,
            output_gate,
            query_down,
            latent_down,
            chain_out,
            attend_out,
        ),
        SP,
        (0, 0, 0, 0, 0, 0, 0, 1, 1),
    )
    (
        full_query,
        full_forward,
        full_backward,
        full_value,
        full_outgate,
        full_query_down,
        full_latent_down,
        full_chain_out,
        full_attend_out,
    ) = gathered
    tok_rows = tokens.shape[0]
    seq_len = tok_rows * lax.axis_size(SP)
    normed = rms_scale(tokens.astype(jnp.float32), input_gain).astype(jnp.bfloat16)

    def project(source, weight):
        return jnp.dot(source, weight, preferred_element_type=jnp.float32).astype(jnp.bfloat16)

    def heads_of(tensor, head_width):
        return tensor.astype(jnp.float32).reshape(
            tok_rows, tensor.shape[1] // head_width, head_width
        )

    def row_term(source, weight):
        return jnp.dot(source, weight, preferred_element_type=jnp.float32)

    query_rows = heads_of(project(normed, full_query), KEY_DIM)
    payload_array_lines = heads_of(project(normed, full_value), VAL_DIM)
    forward_log, forward_key = gate_parts(project(normed, full_forward), forget_rate[0], seq_len)
    backward_log, backward_key = gate_parts(project(normed, full_backward), forget_rate[1], seq_len)
    gate_logit = project(normed, full_outgate).astype(jnp.float32)
    chain_heads = query_rows.shape[1]
    identity = (
        jnp.ones((chain_heads, KEY_DIM), jnp.float32),
        jnp.zeros((chain_heads, KEY_DIM, VAL_DIM), jnp.float32),
    )
    forward_parts = summarize(
        query_rows,
        heads_of(forward_key, KEY_DIM),
        payload_array_lines,
        heads_of(forward_log, KEY_DIM),
    )
    forward_in = carried_in(
        (forward_parts[2], forward_parts[3]), SP, chain_combine, identity, False
    )[1]
    flipped_values = jnp.flip(payload_array_lines, 0)
    backward_parts = summarize(
        jnp.flip(query_rows, 0),
        jnp.flip(heads_of(backward_key, KEY_DIM), 0),
        flipped_values,
        jnp.flip(heads_of(backward_log, KEY_DIM), 0),
    )
    backward_in = carried_in(
        (backward_parts[2], backward_parts[3]), SP, chain_combine, identity, True
    )[1]
    combined = emit(forward_parts[0], forward_parts[1], payload_array_lines, forward_in) + jnp.flip(
        emit(backward_parts[0], backward_parts[1], flipped_values, backward_in), 0
    )
    head_gain = chain_gain.reshape(chain_heads, VAL_DIM)
    chain_mixed = (
        rms_scale(combined, head_gain).reshape(tok_rows, -1) * jax.nn.silu(gate_logit)
    ).astype(jnp.bfloat16)
    raw_query_latent = project(normed, full_query_down)
    raw_pair_latent = project(normed, full_latent_down)
    query_latent = rms_scale(raw_query_latent.astype(jnp.float32), query_latent_gain).astype(
        jnp.bfloat16
    )
    pair_latent = rms_scale(raw_pair_latent.astype(jnp.float32), latent_gain).astype(jnp.bfloat16)
    rotary_key = project(normed, rotary_down).astype(jnp.float32)
    attend_heads = query_up.shape[1] // ATT_QK
    attend_query = (
        project(query_latent, query_up).astype(jnp.float32).reshape(tok_rows, attend_heads, ATT_QK)
    )
    attend_pairs = project(pair_latent, latent_up).reshape(
        tok_rows, attend_heads, NOPE_DIM + VHEAD_DIM
    )
    positions = lax.axis_index(SP) * tok_rows + jnp.arange(tok_rows, dtype=jnp.int32)
    query_final = rotate_tail(rms_scale(attend_query, query_head_gain), positions).astype(
        jnp.bfloat16
    )
    key_cat = jnp.concatenate(
        [
            attend_pairs[..., :NOPE_DIM].astype(jnp.float32),
            jnp.broadcast_to(rotary_key[:, None, :], (tok_rows, attend_heads, ROPE_DIM)),
        ],
        axis=-1,
    )
    key_final = rotate_tail(rms_scale(key_cat, key_head_gain), positions).astype(jnp.bfloat16)
    keys_flat = key_final.reshape(tok_rows, attend_heads * ATT_QK)
    values_flat = attend_pairs[..., NOPE_DIM:].reshape(tok_rows, attend_heads * VHEAD_DIM)
    start_sum = (
        jnp.zeros((tok_rows, attend_heads, VHEAD_DIM), jnp.float32),
        jnp.zeros((attend_heads, tok_rows), jnp.float32),
    )
    pieces = side_by_side((keys_flat, values_flat), SP, 0, 1)
    key_piece = pieces[0].reshape(pieces[0].shape[0], attend_heads, ATT_QK)
    value_piece = pieces[1].reshape(pieces[1].shape[0], attend_heads, VHEAD_DIM)
    piece_rows = key_piece.shape[0]
    span_rows = 1024

    def one_span(partial_sum, interval_couple):
        return (add_scores(partial_sum, query_final, interval_couple[0], interval_couple[1]), None)

    shaped = (
        key_piece.reshape(piece_rows // span_rows, span_rows, attend_heads, ATT_QK),
        value_piece.reshape(piece_rows // span_rows, span_rows, attend_heads, VHEAD_DIM),
    )
    result, _ = lax.scan(one_span, start_sum, shaped)
    numerator, denominator = result
    attend_rows = numerator / jnp.transpose(denominator)[:, :, None]
    attend_mixed = (
        rms_scale(attend_rows, mixer_gain.reshape(attend_heads, VHEAD_DIM))
        .reshape(tok_rows, attend_heads * VHEAD_DIM)
        .astype(jnp.bfloat16)
    )
    return sent_and_summed(
        row_term(chain_mixed, full_chain_out) + row_term(attend_mixed, full_attend_out), "tp", 0
    )


def solution(mesh):
    torus = Mesh(mesh.devices.reshape(8, 4, 2, mesh.shape["tp"]), ("sp_0", "sp_1", "sp_2", "tp"))
    placed = (
        P(SP, None),
        P(),
        P(SP, "tp"),
        P(SP, "tp"),
        P(SP, "tp"),
        P(SP, "tp"),
        P(SP, "tp"),
        P(None, "tp"),
        P("tp"),
        P(SP, None),
        P(SP, None),
        P(),
        P(),
        P(),
        P(None, "tp"),
        P(None, "tp"),
        P(),
        P(),
        P("tp"),
        P("tp", SP),
        P("tp", SP),
    )
    return jax.shard_map(
        on_device, mesh=torus, in_specs=placed, out_specs=P(SP_TP, None), check_vma=False
    )
```

profile of v0, /device:TPU:1, one launch (start us, length us, event | category | flops | bytes accessed | tf_op | source)
XLA Modules:
  0.0 444.4 jit_solution(1386294659774863667)
XLA Ops:
  6.5 0.8 constant_dynamic-update-slice_fusion.8
  10.2 0.8 constant_dynamic-update-slice_fusion.3
  11.0 0.8 constant_dynamic-update-slice_fusion.2
  11.8 0.7 constant_dynamic-update-slice_fusion.1
  14.0 1.3 fusion.11
  15.3 1.6 fusion.44
  16.9 0.7 copy.104
  17.6 1.0 multiply_cosine_fusion
  18.7 89.1 %all-gather.7.cloned.1.call-done = bf16[2048,3072]{1,0:T(8,128)(2,1)} async-done(((bf16[32,3072]{1,0:T(8,128)(2,1)}), bf16[2048,3072]{1,0:T(8,128)(2,1)}) %all-gather.7.cloned.1.call-update) | async-done | bytes 12582928 | tf_op jit(solution)/shard_map/all_gather | solution.py:23
  107.8 1.6 fusion.35
  110.6 1.8 all_gather.66
  112.4 5.8 %all_gather.67 = f32[4,2,128]{2,1,0:T(2,128)S(1)} all-gather(f32[1,2,128]{2,1,0:T(2,128)S(1)} %get-tuple-element.137), channel_id=1, replica_groups=mesh['sp_0'=8,'sp_1'=4,'sp_2'=2,'tp'=4] {'sp_1'}, dimensions={0}, use_global_device_ids=true | all-gather | bytes 5120 | tf_op jit(solution)/shard_map/all_gather | solution.py:42
  118.2 1.6 fusion.40
  120.3 3.7 all_gather.59
  124.1 1.6 fusion.43
  126.7 2.0 all-gather.1
  128.7 2.4 multiply_reduce_fusion.2
  132.1 9.9 %all_gather.71 = f32[4,2,128,128]{3,2,1,0:T(8,128)S(1)} all-gather(f32[1,2,128,128]{3,2,1,0:T(8,128)S(1)} %bitcast_add_fusion.4), channel_id=1, replica_groups=mesh['sp_0'=8,'sp_1'=4,'sp_2'=2,'tp'=4] {'sp_1'}, dimensions={0}, use_global_device_ids=true | all-gather | bytes 655360 | tf_op jit(solution)/shard_map/all_gather | solution.py:42
  142.0 0.9 multiply_add_fusion
  142.9 6.5 %all_gather.60 = f32[4,2,128]{2,1,0:T(2,128)S(1)} all-gather(f32[1,2,128]{2,1,0:T(2,128)S(1)} %get-tuple-element.132), channel_id=1, replica_groups=mesh['sp_0'=8,'sp_1'=4,'sp_2'=2,'tp'=4] {'sp_1'}, dimensions={0}, use_global_device_ids=true | all-gather | bytes 5120 | tf_op jit(solution)/shard_map/all_gather | solution.py:42
  149.9 6.5 %all-gather = f32[4,128,128]{2,1,0:T(8,128)S(1)} all-gather(f32[2,128,128]{2,1,0:T(8,128)S(1)} %convolution_multiply_fusion.4), channel_id=2, replica_groups=mesh['sp_0'=8,'sp_1'=4,'sp_2'=2,'tp'=4] {'sp_2'}, dimensions={0}, use_global_device_ids=true | all-gather | bytes 393216 | tf_op jit(solution)/shard_map/all_gather | solution.py:42
  157.1 10.3 %all_gather.64 = f32[4,2,128,128]{3,2,1,0:T(8,128)S(1)} all-gather(f32[1,2,128,128]{3,2,1,0:T(8,128)S(1)} %bitcast_add_fusion.10), channel_id=1, replica_groups=mesh['sp_0'=8,'sp_1'=4,'sp_2'=2,'tp'=4] {'sp_1'}, dimensions={0}, use_global_device_ids=true | all-gather | bytes 655360 | tf_op jit(solution)/shard_map/all_gather | solution.py:42
  167.5 0.9 multiply_add_fusion.1
  168.5 3.1 multiply_reduce_fusion
  173.8 0.8 subtract_convert_fusion
  176.5 1.9 fusion.42
  178.4 1.4 rev.17
  179.7 11.8 %all_gather.68 = f32[8,2,128]{2,1,0:T(2,128)S(1)} all-gather(f32[1,2,128]{2,1,0:T(2,128)S(1)} %get-tuple-element.126), channel_id=1, replica_groups=mesh['sp_0'=8,'sp_1'=4,'sp_2'=2,'tp'=4] {'sp_0'}, dimensions={0}, use_global_device_ids=true | all-gather | bytes 9216 | tf_op jit(solution)/shard_map/all_gather | solution.py:42
  191.5 10.5 %all_gather.61 = f32[8,2,128]{2,1,0:T(2,128)S(1)} all-gather(f32[1,2,128]{2,1,0:T(2,128)S(1)} %get-tuple-element.121), channel_id=1, replica_groups=mesh['sp_0'=8,'sp_1'=4,'sp_2'=2,'tp'=4] {'sp_0'}, dimensions={0}, use_global_device_ids=true | all-gather | bytes 9216 | tf_op jit(solution)/shard_map/all_gather | solution.py:42
  202.0 0.8 pad_maximum_fusion.3
  203.8 2.4 fusion.76
  206.9 8.0 %all-gather.9.cloned.1.call-done = f32[8,2,128,128]{3,2,1,0:T(8,128)} async-done(((f32[1,2,128,128]{3,2,1,0:T(8,128)}), f32[8,2,128,128]{3,2,1,0:T(8,128)}) %all-gather.9.cloned.1.call-update) | async-done | bytes 1048592 | tf_op jit(solution)/shard_map/all_gather | solution.py:42
  214.9 2.3 fusion.89
  217.7 2.8 fusion.46
  220.4 91.5 %all-gather.13.cloned.1.call-done = bf16[10240,640]{1,0:T(8,128)(2,1)} async-done(((bf16[160,640]{1,0:T(8,128)(2,1)}), bf16[10240,640]{1,0:T(8,128)(2,1)}) %all-gather.13.cloned.1.call-update) | async-done | bytes 13107216 | tf_op jit(solution)/shard_map/all_gather | solution.py:58
  312.0 4.3 split.8
  316.2 8.3 %reshape_reshape.6 = bf16[10,1024,2,128]{3,2,1,0:T(2,128)(2,1)} reshape(bf16[10240,256]{1,0:T(8,128)(2,1)} %split.8) | data formatting | bytes 10485760 | tf_op jit(solution)/shard_map/reshape;reshape | solution.py:304
  324.6 6.9 %split.9 = bf16[10240,384]{1,0:T(8,128)(2,1)} slice(bf16[10240,640]{1,0:T(8,128)(2,1)} %all-gather.13.cloned.1.call-done), slice={[0:10240], [0:384]} | slice | bytes 15728640 | tf_op jit(solution)/shard_map/split | solution.py:58
  331.4 22.6 %reshape_reshape.7 = bf16[10,1024,2,192]{3,2,1,0:T(2,128)(2,1)} reshape(bf16[10240,384]{1,0:T(8,128)(2,1)} %split.9) | data formatting | bytes 15728640 | tf_op jit(solution)/shard_map/reshape;reshape | solution.py:303
  354.1 25.7 %copy.109 = bf16[10,1024,2,192]{1,3,2,0:T(8,128)(2,1)} copy(bf16[10,1024,2,192]{3,2,1,0:T(2,128)(2,1)} %reshape_reshape.7) | data formatting | bytes 15728640
  379.7 34.0 %while.13 = (s32[]{:T(128)}, f32[160,2,128]{2,0,1:T(8,128)S(1)}, f32[2,160]{1,0:T(2,128)S(1)}, bf16[10,1024,2,128]{3,2,1,0:T(2,128)(2,1)}, bf16[10,1024,2,192]{1...) while((s32[]{:T(128)}, f32[160,2,128]{2,0,1:T(8,128)S(1)}, ...), condition=%wide.region_12.13_spmd.clone, body=%wide.region_10.12_spmd.clone.sunk | while | flops 210780480 | bytes 4125808 | solution.py:306
  379.7 1.4 constant_dynamic-slice_fusion.2
  381.2 1.6 fusion.302
  383.1 1.4 constant_dynamic-slice_fusion.2
  384.6 1.6 fusion.302
  386.5 1.4 constant_dynamic-slice_fusion.2
  387.9 1.6 fusion.302
  389.9 1.4 constant_dynamic-slice_fusion.2
  391.3 1.6 fusion.302
  393.3 1.4 constant_dynamic-slice_fusion.2
  394.7 1.6 fusion.302
  396.7 1.4 constant_dynamic-slice_fusion.2
  398.1 1.6 fusion.302
  400.1 1.4 constant_dynamic-slice_fusion.2
  401.5 1.6 fusion.302
  403.5 1.4 constant_dynamic-slice_fusion.2
  404.9 1.6 fusion.302
  406.9 1.4 constant_dynamic-slice_fusion.2
  408.3 1.6 fusion.302
  410.3 1.4 constant_dynamic-slice_fusion.2
  411.7 1.6 fusion.302
  414.0 1.7 convolution_add_fusion
  415.7 21.4 %all_to_all.5 = f32[4,40,2048]{2,1,0:T(8,128)S(1)} all-to-all(f32[4,40,2048]{2,1,0:T(8,128)S(1)} %bitcast.436), channel_id=1, replica_groups=mesh['sp_0'=8,'sp_1'=4,'sp_2'=2,'tp'=4] {'tp'}, dimensions={0} | all-to-all | bytes 2621440 | tf_op jit(solution)/shard_map/all_to_all | solution.py:68
  437.1 0.8 reduce_sum.88
  (175 shorter events, 19.2 us)
Async XLA Ops:
  6.5 165.7 %copy-start = (bf16[768,384]{1,0:T(8,128)(2,1)S(1)}, bf16[768,384]{1,0:T(8,128)(2,1)}, u32[]{:S(2)}) copy-start(bf16[768,384]{1,0:T(8,128)(2,1)} %param.37) | copy-start | bytes 1769476
  6.5 101.2 %all-gather.7.cloned.1.call-start = ((), (), s32[]{:S(2)}) async-start(), calls=%async_computation.1 | async-start | bytes 12779520 | tf_op jit(solution)/shard_map/all_gather | solution.py:23
  11.0 6.6 %copy-start.19 = (f32[2,256]{1,0:T(2,128)S(1)}, f32[2,256]{1,0:T(2,128)}, u32[]{:S(2)}) copy-start(f32[2,256]{1,0:T(2,128)} %param.30) | copy-start | bytes 6148
  13.2 0.7 copy-start.15
  13.2 94.6 %copy-start.6 = (bf16[160,2048]{1,0:T(8,128)(2,1)S(1)}, bf16[160,2048]{1,0:T(8,128)(2,1)}, u32[]{:S(2)}) copy-start(bf16[160,2048]{1,0:T(8,128)(2,1)} %param.23) | copy-start | bytes 1966084
  13.2 94.6 %copy-start.29 = (f32[2048]{0:T(1024)S(1)}, f32[2048]{0:T(1024)}, u32[]{:S(2)}) copy-start(f32[2048]{0:T(1024)} %param.24) | copy-start | bytes 24580
  13.9 189.8 %all-gather.11.cloned.1.call-start = ((), (), s32[]{:S(2)}) async-start(), calls=%async_computation.3 | async-start | bytes 1179648 | tf_op jit(solution)/shard_map/all_gather | solution.py:42
  15.3 153.2 %copy-start.23 = (f32[160]{0:T(256)}, f32[160]{0:T(256)S(1)}, u32[]{:S(2)}) copy-start(f32[160]{0:T(256)S(1)} %add_rsqrt_fusion.6) | copy-start | bytes 1924
  128.7 3.3 copy-start.2
  128.7 2.4 copy-start.7
  128.7 2.4 copy-start.18
  142.9 72.0 %all-gather.9.cloned.1.call-start = ((), (), s32[]{:S(2)}) async-start(), calls=%async_computation.2 | async-start | bytes 1179648 | tf_op jit(solution)/shard_map/all_gather | solution.py:42
  149.9 18.6 %copy-start.30 = (f32[2048]{0:T(1024)S(1)}, f32[2048]{0:T(1024)}, u32[]{:S(2)}) copy-start(f32[2048]{0:T(1024)} %param.24) | copy-start | bytes 24580
  168.4 3.8 copy-start.17
  168.4 143.6 %all-gather.13.cloned.1.call-start = ((), (), s32[]{:S(2)}) async-start(), calls=%async_computation.4 | async-start | bytes 13312000 | tf_op jit(solution)/shard_map/all_gather | solution.py:58
  172.2 1.0 copy-start.12
  172.2 1.2 copy-start.20
  172.6 0.9 copy-start.21
  172.8 0.9 copy-start.8
  172.8 0.9 copy-start.9
  173.6 1.4 copy-start.13
  173.8 2.7 copy-start.24
  173.8 2.7 copy-start.31
  176.4 25.5 %copy-start.10 = (bf16[160,2,32]{2,0,1:T(8,128)(2,1)S(1)}, bf16[160,2,32]{2,0,1:T(8,128)(2,1)}, u32[]{:S(2)}) copy-start(bf16[160,2,32]{2,0,1:T(8,128)(2,1)} %get-tuple-element.97) | copy-start | bytes 61444
  176.4 25.5 %copy-start.11 = (bf16[160,2,32]{2,0,1:T(8,128)(2,1)S(1)}, bf16[160,2,32]{2,0,1:T(8,128)(2,1)}, u32[]{:S(2)}) copy-start(bf16[160,2,32]{2,0,1:T(8,128)(2,1)} %get-tuple-element.98) | copy-start | bytes 61444
  176.4 25.5 %copy-start.14 = (bf16[160,2,128]{2,0,1:T(8,128)(2,1)S(1)}, bf16[160,2,128]{2,0,1:T(8,128)(2,1)}, u32[]{:S(2)}) copy-start(bf16[160,2,128]{2,0,1:T(8,128)(2,1)} %slice.707) | copy-start | bytes 245764
  178.3 24.4 %copy-start.3 = (f32[20,2,8,128]{3,2,1,0:T(8,128)}, f32[20,2,8,128]{3,2,1,0:T(8,128)S(1)}, u32[]{:S(2)}) copy-start(f32[20,2,8,128]{3,2,1,0:T(8,128)S(1)} %fusion.42) | copy-start | bytes 491524
  179.7 23.5 %copy-start.5 = (f32[160,2,128]{2,0,1:T(8,128)S(1)}, f32[160,2,128]{2,0,1:T(8,128)}, u32[]{:S(2)}) copy-start(f32[160,2,128]{2,0,1:T(8,128)} %rev.17) | copy-start | bytes 491524
  202.0 1.7 copy-start.27
  202.0 1.7 copy-start.28
  203.7 11.1 %copy-start.4 = (f32[20,2,8,128]{3,2,1,0:T(8,128)S(1)}, f32[20,2,8,128]{3,2,1,0:T(8,128)}, u32[]{:S(2)}) copy-start(f32[20,2,8,128]{3,2,1,0:T(8,128)} %copy-done.3) | copy-start | bytes 491524
  203.8 11.1 %copy-start.25 = (f32[2,128]{1,0:T(2,128)S(1)}, f32[2,128]{1,0:T(2,128)}, u32[]{:S(2)}) copy-start(f32[2,128]{1,0:T(2,128)} %get-tuple-element.91) | copy-start | bytes 3076
  203.8 11.1 %copy-start.26 = (f32[2,128]{1,0:T(2,128)S(1)}, f32[2,128]{1,0:T(2,128)}, u32[]{:S(2)}) copy-start(f32[2,128]{1,0:T(2,128)} %get-tuple-element.92) | copy-start | bytes 3076
  214.9 2.8 copy-start.32
  214.9 2.8 copy-start.33
  354.1 25.7 %copy-start.16 = (bf16[160,2,192]{2,0,1:T(8,128)(2,1)S(1)}, bf16[160,2,192]{2,0,1:T(8,128)(2,1)}, u32[]{:S(2)}) copy-start(bf16[160,2,192]{2,0,1:T(8,128)(2,1)} %pad_maximum_fusion.3) | copy-start | bytes 368644
  379.7 34.3 %copy-start.22 = (f32[256]{0:T(256)S(1)}, f32[256]{0:T(256)}, u32[]{:S(2)}) copy-start(f32[256]{0:T(256)} %param.41) | copy-start | bytes 3076
  415.7 22.2 %copy-start.1 = (bf16[768,384]{1,0:T(8,128)(2,1)S(1)}, bf16[768,384]{1,0:T(8,128)(2,1)}, u32[]{:S(2)}) copy-start(bf16[768,384]{1,0:T(8,128)(2,1)} %param.37) | copy-start | bytes 1769476
Sparse Core Ops, SparseCore 0:
  14.0 93.7 all-gather.6
  143.0 33.1 all-gather.10
  178.0 36.7 all-gather.8
  217.5 94.4 all-gather.12
where the time goes:
time: 448 us; the launch traced here: 444 us
  waiting for transfers between devices  189 us (42%)
  local copies, waits for them, and re-layouts  95 us (21%)
  blocking collectives  90.2 us (20%)
  matrix products  45.8 us (10%)
  between operations  13.9 us (3%)
  other arithmetic  10.4 us (2%)
    all_gather x1, waiting for transfers between devices, side_by_side(): lax.all_gather(both, axis, axis=dim, tiled=True)  91.5 us
    all_gather x1, waiting for transfers between devices, turned_gather(): filled, at, done = (lax.all_gather(both, axis, axis=0, tiled=True), 0, [])  89.1 us
    all_gather x10, blocking collectives, carried_in(): pieces = jax.tree.map(lambda part: lax.all_gather(part, axis), total)  68.8 us
    unnamed x78, local copies, waits for them, and re-layouts  33.2 us
    another operation x1, local copies, waits for them, and re-layouts, on_device(): key_piece.reshape(piece_rows // span_rows, span_rows, attend_heads, ATT_QK)  22.6 us
    all_to_all x1, blocking collectives, sent_and_summed(): lax.all_to_all(in_blocks(value, dim, count), axis, 0, 0, tiled=True)  21.4 us
    dot_general x10, matrix products, add_scores(): jnp.einsum('qhd,khd->hqk', query_final, key_piece, preferred_element_type...  16 us
    dot_general x9, matrix products, project(): jnp.dot(source, weight, preferred_element_type=jnp.float32)  14.4 us
  transfers between devices with their start and end apart: 4, of which 3 were waited for; matrix products, arithmetic and copies ran while one was open for 6% of the time, Pallas kernels for 0%

commit v1 on v0

--- a/solution.py
+++ b/solution.py
@@ -20,7 +20,13 @@
 def turned_gather(arrays, axis, dims):
     turned = [jnp.moveaxis(a, dim, 0) for a, dim in zip(arrays, dims)]
     both = jnp.concatenate([t.reshape(len(t), -1) for t in turned], axis=1)
-    filled, at, done = (lax.all_gather(both, axis, axis=0, tiled=True), 0, [])
+    filled, at, done = (
+        jnp.concatenate(
+            lax.all_to_all(jnp.stack([both] * lax.axis_size(axis)), axis, 0, 0), axis=0
+        ),
+        0,
+        [],
+    )
     for t, dim in zip(turned, dims):
         share = filled[:, at : at + t[0].size].reshape(-1, *t.shape[1:])
         done.append(jnp.moveaxis(share, 0, dim))

time: 448 us -> 654 us (1.46)
  waiting for transfers between devices: 189 us -> 369 us
  starting transfers between devices: 0.13 us -> 13.6 us
  blocking collectives: 90.2 us -> 97.1 us
    all_to_all x0 -> x1, waiting for transfers between devices: none -> 270 us  [turned_gather(): lax.all_to_all(jnp.stack([both] * lax.axis_size(axis)), axis, 0, 0)]
    all_gather x1 -> x0, waiting for transfers between devices: 89.1 us -> none  [turned_gather(): filled, at, done = (lax.all_gather(both, axis, axis=0, tiled=True), 0, [])]
    all_to_all x0 -> x1, starting transfers between devices: none -> 13.4 us  [turned_gather(): lax.all_to_all(jnp.stack([both] * lax.axis_size(axis)), axis, 0, 0)]
    all_gather x10, blocking collectives: 68.8 us -> 75.7 us  [carried_in(): pieces = jax.tree.map(lambda part: lax.all_gather(part, axis), total)]
    unnamed x78 -> x76, local copies, waits for them, and re-layouts: 33.2 us -> 32.5 us
  transfers between devices with their start and end apart: 4 -> 4, of which waited for: 3 -> 3; matrix products, arithmetic and copies ran while one was open for 6% -> 4% of each run, Pallas kernels for 0% -> 0%
where the time goes in v1:
time: 654 us; the launch traced here: 651 us
  waiting for transfers between devices  369 us (56%)
  local copies, waits for them, and re-layouts  100 us (15%)
  blocking collectives  97.1 us (15%)
  matrix products  47.3 us (7%)
  between operations  13.9 us (2%)
  starting transfers between devices  13.6 us (2%)
  other arithmetic  9.42 us (1%)
    all_to_all x1, waiting for transfers between devices, turned_gather(): lax.all_to_all(jnp.stack([both] * lax.axis_size(axis)), axis, 0, 0)  270 us
    all_gather x1, waiting for transfers between devices, side_by_side(): lax.all_gather(both, axis, axis=dim, tiled=True)  91.6 us
    all_gather x10, blocking collectives, carried_in(): pieces = jax.tree.map(lambda part: lax.all_gather(part, axis), total)  75.7 us
    unnamed x76, local copies, waits for them, and re-layouts  32.5 us
    another operation x1, local copies, waits for them, and re-layouts, on_device(): key_piece.reshape(piece_rows // span_rows, span_rows, attend_heads, ATT_QK)  22.6 us
    all_to_all x1, blocking collectives, sent_and_summed(): lax.all_to_all(in_blocks(value, dim, count), axis, 0, 0, tiled=True)  21.4 us
    dot_general x10, matrix products, add_scores(): jnp.einsum('qhd,khd->hqk', query_final, key_piece, preferred_element_type...  16 us
    dot_general x9, matrix products, project(): jnp.dot(source, weight, preferred_element_type=jnp.float32)  15.9 us
  transfers between devices with their start and end apart: 4, of which 3 were waited for; matrix products, arithmetic and copies ran while one was open for 4% of the time, Pallas kernels for 0%

profile of v1, /device:TPU:1, one launch (start us, length us, event | category | flops | bytes accessed | tf_op | source)
XLA Modules:
  0.0 651.0 jit_solution(11422251342663893181)
XLA Ops:
  6.5 0.8 constant_dynamic-update-slice_fusion.8
  10.2 0.8 constant_dynamic-update-slice_fusion.3
  11.0 0.8 constant_dynamic-update-slice_fusion.2
  13.2 6.1 stack.2
  19.3 13.4 %all-to-all-start = ((bf16[64,32,3072]{2,1,0:T(8,128)(2,1)}), bf16[64,32,3072]{2,1,0:T(8,128)(2,1)}, u32[]{:S(2)}, u32[]{:S(2)}) async-start(bf16[64,32,3072]{2,1,0:T(8,128)(2,1)} %stack.2), calls=%async_computation | async-start | bytes 25165824 | tf_op jit(solution)/shard_map/all_to_all | solution.py:25
  34.3 1.0 multiply_cosine_fusion
  35.3 269.5 %all-to-all-done = bf16[64,32,3072]{2,1,0:T(8,128)(2,1)} async-done(((bf16[64,32,3072]{2,1,0:T(8,128)(2,1)}), bf16[64,32,3072]{2,1,0:T(8,128)(2,1)}, u32[]{:S(2)}, u32[]{:S(2)}) %all-to-all-start) | async-done | bytes 12582944 | tf_op jit(solution)/shard_map/all_to_all | solution.py:25
  304.9 1.6 fusion.43
  306.5 1.7 fusion.35
  308.3 2.2 multiply_reduce_fusion.2
  310.5 1.6 fusion.40
  313.3 5.9 all_gather.62
  319.1 8.1 %all_gather.63 = f32[4,2,128]{2,1,0:T(2,128)S(1)} all-gather(f32[1,2,128]{2,1,0:T(2,128)S(1)} %get-tuple-element.137), channel_id=1, replica_groups=mesh['sp_0'=8,'sp_1'=4,'sp_2'=2,'tp'=4] {'sp_1'}, dimensions={0}, use_global_device_ids=true | all-gather | bytes 5120 | tf_op jit(solution)/shard_map/all_gather | solution.py:48
  327.8 3.8 all_gather.55
  333.0 2.0 all-gather.1
  335.8 9.9 %all_gather.67 = f32[4,2,128,128]{3,2,1,0:T(8,128)S(1)} all-gather(f32[1,2,128,128]{3,2,1,0:T(8,128)S(1)} %bitcast_add_fusion.4), channel_id=1, replica_groups=mesh['sp_0'=8,'sp_1'=4,'sp_2'=2,'tp'=4] {'sp_1'}, dimensions={0}, use_global_device_ids=true | all-gather | bytes 655360 | tf_op jit(solution)/shard_map/all_gather | solution.py:48
  345.7 0.9 multiply_add_fusion
  346.6 1.3 convolution_convert_fusion
  348.0 6.7 %all_gather.56 = f32[4,2,128]{2,1,0:T(2,128)S(1)} all-gather(f32[1,2,128]{2,1,0:T(2,128)S(1)} %get-tuple-element.132), channel_id=1, replica_groups=mesh['sp_0'=8,'sp_1'=4,'sp_2'=2,'tp'=4] {'sp_1'}, dimensions={0}, use_global_device_ids=true | all-gather | bytes 5120 | tf_op jit(solution)/shard_map/all_gather | solution.py:48
  354.7 5.8 all-gather
  361.2 10.3 %all_gather.60 = f32[4,2,128,128]{3,2,1,0:T(8,128)S(1)} all-gather(f32[1,2,128,128]{3,2,1,0:T(8,128)S(1)} %bitcast_add_fusion.10), channel_id=1, replica_groups=mesh['sp_0'=8,'sp_1'=4,'sp_2'=2,'tp'=4] {'sp_1'}, dimensions={0}, use_global_device_ids=true | all-gather | bytes 655360 | tf_op jit(solution)/shard_map/all_gather | solution.py:48
  371.6 0.9 multiply_add_fusion.1
  372.4 3.7 multiply_reduce_fusion
  376.8 1.4 fusion.26
  379.4 0.8 subtract_convert_fusion
  382.1 1.9 fusion.42
  384.0 1.4 rev.17
  385.4 12.8 %all_gather.64 = f32[8,2,128]{2,1,0:T(2,128)S(1)} all-gather(f32[1,2,128]{2,1,0:T(2,128)S(1)} %get-tuple-element.126), channel_id=1, replica_groups=mesh['sp_0'=8,'sp_1'=4,'sp_2'=2,'tp'=4] {'sp_0'}, dimensions={0}, use_global_device_ids=true | all-gather | bytes 9216 | tf_op jit(solution)/shard_map/all_gather | solution.py:48
  398.2 10.4 %all_gather.57 = f32[8,2,128]{2,1,0:T(2,128)S(1)} all-gather(f32[1,2,128]{2,1,0:T(2,128)S(1)} %get-tuple-element.121), channel_id=1, replica_groups=mesh['sp_0'=8,'sp_1'=4,'sp_2'=2,'tp'=4] {'sp_0'}, dimensions={0}, use_global_device_ids=true | all-gather | bytes 9216 | tf_op jit(solution)/shard_map/all_gather | solution.py:48
  408.7 0.8 pad_maximum_fusion.3
  410.4 2.4 fusion.76
  413.5 7.7 %all-gather.6.cloned.1.call-done = f32[8,2,128,128]{3,2,1,0:T(8,128)} async-done(((f32[1,2,128,128]{3,2,1,0:T(8,128)}), f32[8,2,128,128]{3,2,1,0:T(8,128)}) %all-gather.6.cloned.1.call-update) | async-done | bytes 1048592 | tf_op jit(solution)/shard_map/all_gather | solution.py:48
  421.3 2.3 fusion.89
  424.1 2.8 fusion.46
  426.9 91.6 %all-gather.10.cloned.1.call-done = bf16[10240,640]{1,0:T(8,128)(2,1)} async-done(((bf16[160,640]{1,0:T(8,128)(2,1)}), bf16[10240,640]{1,0:T(8,128)(2,1)}) %all-gather.10.cloned.1.call-update) | async-done | bytes 13107216 | tf_op jit(solution)/shard_map/all_gather | solution.py:64
  518.5 4.3 split.8
  522.8 8.3 %reshape_reshape.6 = bf16[10,1024,2,128]{3,2,1,0:T(2,128)(2,1)} reshape(bf16[10240,256]{1,0:T(8,128)(2,1)} %split.8) | data formatting | bytes 10485760 | tf_op jit(solution)/shard_map/reshape;reshape | solution.py:310
  531.1 6.9 %split.9 = bf16[10240,384]{1,0:T(8,128)(2,1)} slice(bf16[10240,640]{1,0:T(8,128)(2,1)} %all-gather.10.cloned.1.call-done), slice={[0:10240], [0:384]} | slice | bytes 15728640 | tf_op jit(solution)/shard_map/split | solution.py:64
  538.0 22.6 %reshape_reshape.7 = bf16[10,1024,2,192]{3,2,1,0:T(2,128)(2,1)} reshape(bf16[10240,384]{1,0:T(8,128)(2,1)} %split.9) | data formatting | bytes 15728640 | tf_op jit(solution)/shard_map/reshape;reshape | solution.py:309
  560.6 25.7 %copy.109 = bf16[10,1024,2,192]{1,3,2,0:T(8,128)(2,1)} copy(bf16[10,1024,2,192]{3,2,1,0:T(2,128)(2,1)} %reshape_reshape.7) | data formatting | bytes 15728640
  586.3 34.0 %while.13 = (s32[]{:T(128)}, f32[160,2,128]{2,0,1:T(8,128)S(1)}, f32[2,160]{1,0:T(2,128)S(1)}, bf16[10,1024,2,128]{3,2,1,0:T(2,128)(2,1)}, bf16[10,1024,2,192]{1...) while((s32[]{:T(128)}, f32[160,2,128]{2,0,1:T(8,128)S(1)}, ...), condition=%wide.region_12.13_spmd.clone, body=%wide.region_10.12_spmd.clone.sunk | while | flops 210780480 | bytes 4125808 | solution.py:312
  586.3 1.4 constant_dynamic-slice_fusion.2
  587.7 1.6 fusion.302
  589.7 1.4 constant_dynamic-slice_fusion.2
  591.1 1.6 fusion.302
  593.1 1.4 constant_dynamic-slice_fusion.2
  594.5 1.6 fusion.302
  596.5 1.4 constant_dynamic-slice_fusion.2
  597.9 1.6 fusion.302
  599.9 1.4 constant_dynamic-slice_fusion.2
  601.3 1.6 fusion.302
  603.3 1.4 constant_dynamic-slice_fusion.2
  604.7 1.6 fusion.302
  606.7 1.4 constant_dynamic-slice_fusion.2
  608.1 1.6 fusion.302
  610.1 1.4 constant_dynamic-slice_fusion.2
  611.5 1.6 fusion.302
  613.5 1.4 constant_dynamic-slice_fusion.2
  614.9 1.6 fusion.302
  616.9 1.4 constant_dynamic-slice_fusion.2
  618.3 1.6 fusion.302
  620.5 1.7 convolution_add_fusion
  622.3 21.4 %all_to_all.10 = f32[4,40,2048]{2,1,0:T(8,128)S(1)} all-to-all(f32[4,40,2048]{2,1,0:T(8,128)S(1)} %bitcast.437), channel_id=1, replica_groups=mesh['sp_0'=8,'sp_1'=4,'sp_2'=2,'tp'=4] {'tp'}, dimensions={0} | all-to-all | bytes 2621440 | tf_op jit(solution)/shard_map/all_to_all | solution.py:74
  643.7 0.8 reduce_sum.88
  (173 shorter events, 19.9 us)
Async XLA Ops:
  6.5 370.3 %copy-start = (bf16[768,384]{1,0:T(8,128)(2,1)S(1)}, bf16[768,384]{1,0:T(8,128)(2,1)}, u32[]{:S(2)}) copy-start(bf16[768,384]{1,0:T(8,128)(2,1)} %param.37) | copy-start | bytes 1769476
  19.3 13.5 %copy-start.6 = (bf16[160,2048]{1,0:T(8,128)(2,1)S(1)}, bf16[160,2048]{1,0:T(8,128)(2,1)}, u32[]{:S(2)}) copy-start(bf16[160,2048]{1,0:T(8,128)(2,1)} %param.23) | copy-start | bytes 1966084
  19.3 13.8 %copy-start.27 = (bf16[2048,64]{0,1:T(8,128)(2,1)S(1)}, bf16[2048,64]{0,1:T(8,128)(2,1)}, u32[]{:S(2)}) copy-start(bf16[2048,64]{0,1:T(8,128)(2,1)} %param.34) | copy-start | bytes 786436
  19.3 13.8 %copy-start.28 = (f32[2048]{0:T(1024)S(1)}, f32[2048]{0:T(1024)}, u32[]{:S(2)}) copy-start(f32[2048]{0:T(1024)} %param.24) | copy-start | bytes 24580
  19.3 285.6 %all-to-all-start = ((bf16[64,32,3072]{2,1,0:T(8,128)(2,1)}), bf16[64,32,3072]{2,1,0:T(8,128)(2,1)}, u32[]{:S(2)}, u32[]{:S(2)}) async-start(bf16[64,32,3072]{2,1,0:T(8,128)(2,1)} %stack.2), calls=%async_computation | async-start | bytes 25165824 | tf_op jit(solution)/shard_map/all_to_all | solution.py:25
  32.8 1.5 copy-start.17
  32.8 377.6 %all-gather.8.cloned.1.call-start = ((), (), s32[]{:S(2)}) async-start(), calls=%async_computation.3 | async-start | bytes 1179648 | tf_op jit(solution)/shard_map/all_gather | solution.py:48
  33.1 339.3 %copy-start.21 = (f32[160]{0:T(256)}, f32[160]{0:T(256)S(1)}, u32[]{:S(2)}) copy-start(f32[160]{0:T(256)S(1)} %add_rsqrt_fusion.6) | copy-start | bytes 1924
  332.4 14.2 %copy-start.16 = (f32[512]{0:T(512)S(1)}, f32[512]{0:T(512)}, u32[]{:S(2)}) copy-start(f32[512]{0:T(512)} %param.36) | copy-start | bytes 6148
  335.0 12.9 %copy-start.2 = (f32[4,128,128]{2,1,0:T(8,128)}, f32[4,128,128]{2,1,0:T(8,128)S(1)}, u32[]{:S(2)}) copy-start(f32[4,128,128]{2,1,0:T(8,128)S(1)} %all-gather.1) | copy-start | bytes 786436
  346.6 74.7 %all-gather.6.cloned.1.call-start = ((), (), s32[]{:S(2)}) async-start(), calls=%async_computation.2 | async-start | bytes 1179648 | tf_op jit(solution)/shard_map/all_gather | solution.py:48
  348.0 24.4 %copy-start.29 = (f32[2048]{0:T(1024)S(1)}, f32[2048]{0:T(1024)}, u32[]{:S(2)}) copy-start(f32[2048]{0:T(1024)} %param.24) | copy-start | bytes 24580
  372.4 4.4 copy-start.15
  376.1 142.4 %all-gather.10.cloned.1.call-start = ((), (), s32[]{:S(2)}) async-start(), calls=%async_computation.4 | async-start | bytes 13312000 | tf_op jit(solution)/shard_map/all_gather | solution.py:64
  376.8 2.1 copy-start.11
  376.8 2.3 copy-start.18
  378.2 0.9 copy-start.19
  378.5 0.9 copy-start.7
  378.5 0.9 copy-start.8
  379.3 1.4 copy-start.12
  379.4 2.7 copy-start.22
  379.4 2.7 copy-start.30
  382.1 26.5 %copy-start.9 = (bf16[160,2,32]{2,0,1:T(8,128)(2,1)S(1)}, bf16[160,2,32]{2,0,1:T(8,128)(2,1)}, u32[]{:S(2)}) copy-start(bf16[160,2,32]{2,0,1:T(8,128)(2,1)} %get-tuple-element.97) | copy-start | bytes 61444
  382.1 26.5 %copy-start.10 = (bf16[160,2,32]{2,0,1:T(8,128)(2,1)S(1)}, bf16[160,2,32]{2,0,1:T(8,128)(2,1)}, u32[]{:S(2)}) copy-start(bf16[160,2,32]{2,0,1:T(8,128)(2,1)} %get-tuple-element.98) | copy-start | bytes 61444
  382.1 26.5 %copy-start.13 = (bf16[160,2,128]{2,0,1:T(8,128)(2,1)S(1)}, bf16[160,2,128]{2,0,1:T(8,128)(2,1)}, u32[]{:S(2)}) copy-start(bf16[160,2,128]{2,0,1:T(8,128)(2,1)} %slice.707) | copy-start | bytes 245764
  384.0 25.4 %copy-start.3 = (f32[20,2,8,128]{3,2,1,0:T(8,128)}, f32[20,2,8,128]{3,2,1,0:T(8,128)S(1)}, u32[]{:S(2)}) copy-start(f32[20,2,8,128]{3,2,1,0:T(8,128)S(1)} %fusion.42) | copy-start | bytes 491524
  385.4 24.5 %copy-start.5 = (f32[160,2,128]{2,0,1:T(8,128)S(1)}, f32[160,2,128]{2,0,1:T(8,128)}, u32[]{:S(2)}) copy-start(f32[160,2,128]{2,0,1:T(8,128)} %rev.17) | copy-start | bytes 491524
  408.6 1.7 copy-start.25
  408.6 1.7 copy-start.26
  410.4 10.9 %copy-start.4 = (f32[20,2,8,128]{3,2,1,0:T(8,128)S(1)}, f32[20,2,8,128]{3,2,1,0:T(8,128)}, u32[]{:S(2)}) copy-start(f32[20,2,8,128]{3,2,1,0:T(8,128)} %copy-done.3) | copy-start | bytes 491524
  410.4 10.9 %copy-start.23 = (f32[2,128]{1,0:T(2,128)S(1)}, f32[2,128]{1,0:T(2,128)}, u32[]{:S(2)}) copy-start(f32[2,128]{1,0:T(2,128)} %get-tuple-element.91) | copy-start | bytes 3076
  410.4 10.9 %copy-start.24 = (f32[2,128]{1,0:T(2,128)S(1)}, f32[2,128]{1,0:T(2,128)}, u32[]{:S(2)}) copy-start(f32[2,128]{1,0:T(2,128)} %get-tuple-element.92) | copy-start | bytes 3076
  421.3 2.8 copy-start.31
  421.3 2.8 copy-start.32
  560.6 25.7 %copy-start.14 = (bf16[160,2,192]{2,0,1:T(8,128)(2,1)S(1)}, bf16[160,2,192]{2,0,1:T(8,128)(2,1)}, u32[]{:S(2)}) copy-start(bf16[160,2,192]{2,0,1:T(8,128)(2,1)} %pad_maximum_fusion.3) | copy-start | bytes 368644
  586.3 34.2 %copy-start.20 = (f32[256]{0:T(256)S(1)}, f32[256]{0:T(256)}, u32[]{:S(2)}) copy-start(f32[256]{0:T(256)} %param.41) | copy-start | bytes 3076
  622.3 22.2 %copy-start.1 = (bf16[768,384]{1,0:T(8,128)(2,1)S(1)}, bf16[768,384]{1,0:T(8,128)(2,1)}, u32[]{:S(2)}) copy-start(bf16[768,384]{1,0:T(8,128)(2,1)} %param.37) | copy-start | bytes 1769476
Sparse Core Ops, SparseCore 0:
  346.7 36.6 all-gather.7
  385.1 36.1 all-gather.5
  424.0 94.4 all-gather.9
